TPU v7x, 32 devices: a whole 2x2x4 slice. The times are simulated.
32 devices in a mesh: grp: 2 (over y), fs: 4 (over z), tp: 4 (over x, core).
Axes of the slice: x: 2, y: 2, z: 4, core: 2. Of those that a mesh axis runs over, the one named last changes fastest.
Arguments:
- prompt: bfloat16 [2048, 2048], P(('grp', 'tp')), parts along dimension 0, may hold values from -6 to 6
- gain_first: float32 [2048], P('fs'), may hold values from 0.1 to 1.9
- gate_first: float32 [2048, 4096], P('fs', 'tp'), may hold values from -0.125 to 0.125
- up_first: float32 [2048, 4096], P('fs', 'tp'), may hold values from -0.125 to 0.125
- down_first: float32 [4096, 2048], P('fs', 'tp'), may hold values from -0.09375 to 0.09375
- gain_second: float32 [2048], P('fs'), may hold values from 0.1 to 1.9
- gate_second: float32 [2048, 4096], P('fs', 'tp'), may hold values from -0.125 to 0.125
- up_second: float32 [2048, 4096], P('fs', 'tp'), may hold values from -0.125 to 0.125
- down_second: float32 [4096, 2048], P('fs', 'tp'), may hold values from -0.09375 to 0.09375
Outputs:
- result: bfloat16 [2048, 2048], P(('grp', 'tp')), parts along dimension 0
- served_gate_first: bfloat16 [4096, 4096], P('grp', 'fs'), parts along dimension 0
- served_up_first: bfloat16 [4096, 4096], P('grp', 'fs'), parts along dimension 0
- served_down_first: bfloat16 [4096, 4096], P('fs', 'grp'), parts along dimension 1
- served_gate_second: bfloat16 [4096, 4096], P('grp', 'fs'), parts along dimension 0
- served_up_second: bfloat16 [4096, 4096], P('grp', 'fs'), parts along dimension 0
- served_down_second: bfloat16 [4096, 4096], P('fs', 'grp'), parts along dimension 1
There are 2 independent parts, one for each index of `grp`. A program takes and returns all parts, laid end to end along the dimension named above; an argument that names none is the same for every part. Nothing has to cross between parts.
All inputs are finite; a program needn't handle non-finite values.
Results may differ from a plain program's by a relative error of at most 0.0053.
Values may be sent and summed in bfloat16 or wider, within the bound.
A program may use at most 128 MiB of HBM per device.

v0:
```python
import jax
import jax.numpy as jnp
from jax import lax
from jax.sharding import PartitionSpec as P

EPS = 1e-06


def as_sent(array):
    return jax.tree.map(lambda a: a.astype(jnp.bfloat16) if a.dtype == jnp.float32 else a, array)


def fold(gain, weight):
    return (gain[:, None] * weight).astype(jnp.bfloat16)


def normed_of(stream):
    return (stream * lax.rsqrt(jnp.mean(stream * stream, axis=-1, keepdims=True) + EPS)).astype(
        jnp.bfloat16
    )


def hidden_of(normed, w_gate, w_up):
    gate = jnp.dot(normed, w_gate, preferred_element_type=jnp.float32)
    up_val = jnp.dot(normed, w_up, preferred_element_type=jnp.float32)
    return (jax.nn.silu(gate) * up_val).astype(jnp.bfloat16)


def on_device(
    prompt,
    gain_first,
    gate_first,
    up_first,
    down_first,
    gain_second,
    gate_second,
    up_second,
    down_second,
):
    folded = (
        fold(gain_first, gate_first),
        fold(gain_first, up_first),
        fold(gain_second, gate_second),
        fold(gain_second, up_second),
    )
    downs = (down_first.astype(jnp.bfloat16), down_second.astype(jnp.bfloat16))
    spread = (
        lax.all_to_all(folded[0], "tp", split_axis=0, concat_axis=1, tiled=True),
        lax.all_to_all(folded[1], "tp", split_axis=0, concat_axis=1, tiled=True),
        lax.all_to_all(folded[2], "tp", split_axis=0, concat_axis=1, tiled=True),
        lax.all_to_all(folded[3], "tp", split_axis=0, concat_axis=1, tiled=True),
    )
    moved = (
        lax.all_to_all(spread[0], "fs", split_axis=1, concat_axis=0, tiled=True),
        lax.all_to_all(spread[1], "fs", split_axis=1, concat_axis=0, tiled=True),
        lax.all_to_all(spread[2], "fs", split_axis=1, concat_axis=0, tiled=True),
        lax.all_to_all(spread[3], "fs", split_axis=1, concat_axis=0, tiled=True),
    )
    n_fs = lax.axis_size("fs")
    width = moved[0].shape[1]
    piece = moved[0].shape[0] // n_fs
    shaped = tuple((m.reshape(n_fs, piece, width) for m in moved))
    joined = jax.tree.map(
        lambda part, own: part.astype(own.dtype),
        lax.all_gather(as_sent(shaped), "tp", axis=1, tiled=True),
        shaped,
    )
    served = tuple((m.reshape(-1, width) for m in joined))
    served_downs = (
        lax.all_gather(downs[0], "tp", axis=1, tiled=True),
        lax.all_gather(downs[1], "tp", axis=1, tiled=True),
    )
    gates = (served[0], served[2])
    ups = (served[1], served[3])
    stream = prompt.astype(jnp.float32)
    for layer in range(2):
        hidden = hidden_of(normed_of(stream), gates[layer], ups[layer])
        partial_out = jnp.dot(hidden, served_downs[layer], preferred_element_type=jnp.float32)
        stream = stream + 0.5 * lax.psum(partial_out, "fs")
    result = stream.astype(jnp.bfloat16)
    return (result, served[0], served[1], served_downs[0], served[2], served[3], served_downs[1])


def solution(mesh):
    return jax.shard_map(
        on_device,
        mesh=mesh,
        in_specs=(
            P(("grp", "tp"), None),
            P("fs"),
            P("fs", "tp"),
            P("fs", "tp"),
            P("fs", "tp"),
            P("fs"),
            P("fs", "tp"),
            P("fs", "tp"),
            P("fs", "tp"),
        ),
        out_specs=(
            P(("grp", "tp"), None),
            P("grp", "fs"),
            P("grp", "fs"),
            P("fs", "grp"),
            P("grp", "fs"),
            P("grp", "fs"),
            P("fs", "grp"),
        ),
        check_vma=False,
    )
```

profile of v0, /device:TPU:0, one launch (start us, length us, event | category | flops | bytes accessed | tf_op | source)
XLA Modules:
  0.0 552.0 jit_solution(7371921522746309)
XLA Ops:
  7.2 2.5 multiply_convert_fusion.4
  9.7 18.5 %all_to_all.116 = bf16[4,128,1024]{2,1,0:T(8,128)(2,1)S(1)} all-to-all(bf16[4,128,1024]{2,1,0:T(8,128)(2,1)S(1)} %bitcast.43), channel_id=1, replica_groups=mesh['grp'=2,'fs'=4,'tp'=4] {'tp'}, dimensions={0} | all-to-all | bytes 2097152 | tf_op jit(solution)/shard_map/all_to_all | solution.py:48
  28.2 30.1 %all_to_all.117 = bf16[128,4,1024]{2,0,1:T(8,128)(2,1)} all-to-all(bf16[128,4,1024]{2,0,1:T(8,128)(2,1)S(1)} %bitcast.37), channel_id=1, replica_groups=mesh['grp'=2,'fs'=4,'tp'=4] {'fs'}, dimensions={1} | all-to-all | bytes 2097152 | tf_op jit(solution)/shard_map/all_to_all | solution.py:54
  58.4 2.7 convert_element_type.41
  61.2 28.0 %all_to_all.118 = bf16[4,128,1024]{2,1,0:T(8,128)(2,1)S(1)} all-to-all(bf16[4,128,1024]{2,1,0:T(8,128)(2,1)S(1)} %bitcast.42), channel_id=1, replica_groups=mesh['grp'=2,'fs'=4,'tp'=4] {'tp'}, dimensions={0} | all-to-all | bytes 2097152 | tf_op jit(solution)/shard_map/all_to_all | solution.py:49
  89.2 28.6 %all_to_all.119 = bf16[128,4,1024]{2,0,1:T(8,128)(2,1)} all-to-all(bf16[128,4,1024]{2,0,1:T(8,128)(2,1)S(1)} %bitcast.38), channel_id=1, replica_groups=mesh['grp'=2,'fs'=4,'tp'=4] {'fs'}, dimensions={1} | all-to-all | bytes 2097152 | tf_op jit(solution)/shard_map/all_to_all | solution.py:55
  117.9 3.5 multiply_convert_fusion.1
  121.4 3.6 all-to-all-start.4
  125.4 4.5 fusion.10
  129.9 14.3 %all-gather.11.cloned.1.call-done = bf16[1024,2048]{1,0:T(8,128)(2,1)} async-done(((bf16[1024,512]{1,0:T(8,128)(2,1)}), bf16[1024,2048]{1,0:T(8,128)(2,1)}) %all-gather.11.cloned.1.call-update) | async-done | bytes 4194320 | tf_op jit(solution)/shard_map/all_gather | solution.py:70
  144.1 38.1 %all-gather.9.cloned.1.call-done = bf16[4,512,1024]{2,1,0:T(8,128)(2,1)} async-done(((bf16[4,128,1024]{2,1,0:T(8,128)(2,1)}), bf16[4,512,1024]{2,1,0:T(8,128)(2,1)}) %all-gather.9.cloned.1.call-update) | async-done | bytes 4194320 | tf_op jit(solution)/shard_map/all_gather | solution.py:65
  182.2 7.6 %fusion.5 = f32[256,2048]{1,0:T(8,128)} fusion(bf16[1024,2048]{1,0:T(8,128)(2,1)} %all-gather.11.cloned.1.call-done, bf16[2048,1024]{1,0:T(8,128)(2,1)} %bitcast.26, f32[256,1024]{1,0:T(8,128)} %fusion.10, bf16[256,2048]{1,0:T(8,128)(2,1)S(1)} %copy-done.1, f32[256]{0:T(256)S(1)} %add_rsqrt_fusion.1), kind=kOutput, calls=%fused_computation.17 | convolution fusion | flops 2150629376 | bytes 12583936 | tf_op jit(solution)/shard_map/dot_general | solution.py:78
  189.9 57.0 %all_to_all.120 = bf16[128,4,1024]{2,0,1:T(8,128)(2,1)} all-to-all(bf16[128,4,1024]{2,0,1:T(8,128)(2,1)S(1)} %bitcast.34), channel_id=1, replica_groups=mesh['grp'=2,'fs'=4,'tp'=4] {'fs'}, dimensions={1} | all-to-all | bytes 2097152 | tf_op jit(solution)/shard_map/all_to_all | solution.py:56
  247.0 2.7 convert_element_type.46
  249.8 16.9 %all_to_all.121 = bf16[4,128,1024]{2,1,0:T(8,128)(2,1)S(1)} all-to-all(bf16[4,128,1024]{2,1,0:T(8,128)(2,1)S(1)} %bitcast.40), channel_id=1, replica_groups=mesh['grp'=2,'fs'=4,'tp'=4] {'tp'}, dimensions={0} | all-to-all | bytes 2097152 | tf_op jit(solution)/shard_map/all_to_all | solution.py:51
  266.6 52.7 %all_to_all.122 = bf16[128,4,1024]{2,0,1:T(8,128)(2,1)} all-to-all(bf16[128,4,1024]{2,0,1:T(8,128)(2,1)S(1)} %bitcast.39), channel_id=1, replica_groups=mesh['grp'=2,'fs'=4,'tp'=4] {'fs'}, dimensions={1} | all-to-all | bytes 2097152 | tf_op jit(solution)/shard_map/all_to_all | solution.py:57
  319.9 2.2 multiply_reduce_fusion
  323.4 31.3 %all-gather.13.cloned.1.call-done = bf16[4,512,1024]{2,1,0:T(8,128)(2,1)} async-done(((bf16[4,128,1024]{2,1,0:T(8,128)(2,1)}), bf16[4,512,1024]{2,1,0:T(8,128)(2,1)}) %all-gather.13.cloned.1.call-update) | async-done | bytes 4194320 | tf_op jit(solution)/shard_map/all_gather | solution.py:65
  354.7 4.7 fusion.14
  359.4 31.7 %all-gather.17.cloned.1.call-done = bf16[1024,2048]{1,0:T(8,128)(2,1)} async-done(((bf16[1024,512]{1,0:T(8,128)(2,1)}), bf16[1024,2048]{1,0:T(8,128)(2,1)}) %all-gather.17.cloned.1.call-update) | async-done | bytes 4194320 | tf_op jit(solution)/shard_map/all_gather | solution.py:71
  391.2 36.0 %all-gather.15.cloned.1.call-done = bf16[4,512,1024]{2,1,0:T(8,128)(2,1)} async-done(((bf16[4,128,1024]{2,1,0:T(8,128)(2,1)}), bf16[4,512,1024]{2,1,0:T(8,128)(2,1)}) %all-gather.15.cloned.1.call-update) | async-done | bytes 4194320 | tf_op jit(solution)/shard_map/all_gather | solution.py:65
  427.2 7.9 %fusion.4 = f32[256,2048]{1,0:T(8,128)} fusion(bf16[1024,2048]{1,0:T(8,128)(2,1)} %all-gather.17.cloned.1.call-done, bf16[256,2048]{1,0:T(8,128)(2,1)} %multiply_convert_fusion.2, bf16[2048,1024]{1,0:T(8,128)(2,1)} %bitcast.30, f32[256,1024]{1,0:T(8,128)} %fusion.14), kind=kOutput, calls=%fused_computation.16 | convolution fusion | flops 2149056512 | bytes 12582912 | tf_op jit(solution)/shard_map/dot_general | solution.py:78
  435.1 86.3 %all-reduce.5.cloned.1.call-done = f32[256,2048]{1,0:T(8,128)} async-done(((f32[256,2048]{1,0:T(8,128)}), f32[256,2048]{1,0:T(8,128)}) %all-reduce.5.cloned.1.call-update) | async-done | bytes 2097168 | tf_op jit(solution)/shard_map/psum | solution.py:79
  521.4 3.2 add_convert_fusion
  524.6 2.1 copy.24
  526.8 1.6 copy-done.4
  528.3 2.1 copy.25
  530.5 1.6 copy-done.3
  532.0 2.1 copy.26
  535.7 2.1 copy.27
  539.4 2.1 copy.28
  543.1 2.0 copy.29
  (39 shorter events, 7.3 us)
Async XLA Ops:
  7.2 118.2 %all-gather.7.cloned.1.call-start = ((), (), s32[]{:S(2)}) async-start(), calls=%async_computation.8 | async-start | bytes 5242880 | tf_op jit(solution)/shard_map/all_gather | solution.py:65
  58.4 85.8 %all-gather.11.cloned.1.call-start = ((), (), s32[]{:S(2)}) async-start(), calls=%async_computation.10 | async-start | bytes 5242880 | tf_op jit(solution)/shard_map/all_gather | solution.py:70
  61.1 121.1 %all-gather.9.cloned.1.call-start = ((), (), s32[]{:S(2)}) async-start(), calls=%async_computation.9 | async-start | bytes 5242880 | tf_op jit(solution)/shard_map/all_gather | solution.py:65
  89.2 28.6 %copy-start.8 = (f32[512]{0:T(512)S(1)}, f32[512]{0:T(512)}, u32[]{:S(2)}) copy-start(f32[512]{0:T(512)} %param.14) | copy-start | bytes 6148
  121.4 3.7 copy-start.1
  121.4 68.6 %all-to-all-start.4 = ((bf16[4,128,1024]{2,1,0:T(8,128)(2,1)}), bf16[4,128,1024]{2,1,0:T(8,128)(2,1)S(1)}, u32[]{:S(2)}, u32[]{:S(2)}) async-start(bf16[4,128,1024]{2,1,0:T(8,128)(2,1)} %bitcast.41), calls=%async_computation.4 | async-start | bytes 2097152 | tf_op jit(solution)/shard_map/all_to_all | solution.py:50
  125.0 194.8 %all-reduce.3.cloned.1.call-start = ((), (), s32[]{:S(2)}) async-start(), calls=%async_computation.11 | async-start | bytes 4194304 | tf_op jit(solution)/shard_map/psum | solution.py:79
  189.9 164.8 %all-gather.13.cloned.1.call-start = ((), (), s32[]{:S(2)}) async-start(), calls=%async_computation.12 | async-start | bytes 5242880 | tf_op jit(solution)/shard_map/all_gather | solution.py:65
  246.9 144.2 %all-gather.17.cloned.1.call-start = ((), (), s32[]{:S(2)}) async-start(), calls=%async_computation.14 | async-start | bytes 5242880 | tf_op jit(solution)/shard_map/all_gather | solution.py:71
  249.7 177.5 %all-gather.15.cloned.1.call-start = ((), (), s32[]{:S(2)}) async-start(), calls=%async_computation.13 | async-start | bytes 5242880 | tf_op jit(solution)/shard_map/all_gather | solution.py:65
  319.3 202.1 %all-reduce.5.cloned.1.call-start = ((), (), s32[]{:S(2)}) async-start(), calls=%async_computation.15 | async-start | bytes 4194304 | tf_op jit(solution)/shard_map/psum | solution.py:79
  319.9 2.2 copy-start
  521.4 3.2 copy-start.2
  524.6 3.7 copy-start.4
  528.3 3.7 copy-start.3
  532.0 3.7 copy-start.5
  535.7 3.7 copy-start.7
  539.4 3.7 copy-start.6
Sparse Core Ops, SparseCore 0:
  58.5 43.5 all-gather.6
  104.3 39.8 all-gather.10
  145.7 36.5 all-gather.8
  190.0 129.8 all-reduce.2
  321.3 33.3 all-gather.12
  356.7 34.4 all-gather.16
  392.7 34.4 all-gather.14
  435.2 86.1 all-reduce.4
where the time goes:
time: 553 us; the launch traced here: 552 us
  waiting for transfers between devices  238 us (43%)
  blocking collectives  232 us (42%)
  matrix products  24.7 us (4%)
  local copies, waits for them, and re-layouts  20.6 us (4%)
  other arithmetic  18.4 us (3%)
  between operations  14.2 us (3%)
    all_gather x4, waiting for transfers between devices, on_device(): lax.all_gather(as_sent(shaped), 'tp', axis=1, tiled=True)  106 us
    psum x2, waiting for transfers between devices, on_device(): stream = stream + 0.5 * lax.psum(partial_out, 'fs')  86.8 us
    all_to_all x1, blocking collectives, on_device(): lax.all_to_all(spread[2], 'fs', split_axis=1, concat_axis=0, tiled=True)  57 us
    all_to_all x1, blocking collectives, on_device(): lax.all_to_all(spread[3], 'fs', split_axis=1, concat_axis=0, tiled=True)  52.7 us
    all_gather x1, waiting for transfers between devices, on_device(): lax.all_gather(downs[1], 'tp', axis=1, tiled=True)  31.7 us
    all_to_all x1, blocking collectives, on_device(): lax.all_to_all(spread[0], 'fs', split_axis=1, concat_axis=0, tiled=True)  30.1 us
    all_to_all x1, blocking collectives, on_device(): lax.all_to_all(spread[1], 'fs', split_axis=1, concat_axis=0, tiled=True)  28.6 us
    all_to_all x1, blocking collectives, on_device(): lax.all_to_all(folded[1], 'tp', split_axis=0, concat_axis=1, tiled=True)  28 us
  transfers between devices with their start and end apart: 9, of which 7 were waited for; matrix products, arithmetic and copies ran while one was open for 5% of the time, Pallas kernels for 0%

commit v1 on v0

--- a/solution.py
+++ b/solution.py
@@ -76,7 +76,7 @@
     for layer in range(2):
         hidden = hidden_of(normed_of(stream), gates[layer], ups[layer])
         partial_out = jnp.dot(hidden, served_downs[layer], preferred_element_type=jnp.float32)
-        stream = stream + 0.5 * lax.psum(partial_out, "fs")
+        stream = stream + 0.5 * jnp.sum(lax.all_gather(partial_out, "fs"), axis=0)
     result = stream.astype(jnp.bfloat16)
     return (result, served[0], served[1], served_downs[0], served[2], served[3], served_downs[1])
 

time: 553 us -> 675 us (1.22)
  waiting for transfers between devices: 238 us -> 333 us
  blocking collectives: 232 us -> 257 us
    all_gather x0 -> x2, waiting for transfers between devices: none -> 184 us  [on_device(): stream = stream + 0.5 * jnp.sum(lax.all_gather(partial_out, 'fs'), axis=0)]
    psum x2 -> x0, waiting for transfers between devices: 86.8 us -> none  [on_device(): stream = stream + 0.5 * lax.psum(partial_out, 'fs')]
    all_to_all x0 -> x1, blocking collectives: none -> 16.9 us  [on_device(): lax.all_to_all(folded[2], 'tp', split_axis=0, concat_axis=1, tiled=True)]
    reduce_sum x0 -> x2, other arithmetic: none -> 10.1 us  [on_device(): stream = stream + 0.5 * jnp.sum(lax.all_gather(partial_out, 'fs'), axis=0)]
  transfers between devices with their start and end apart: 9 -> 8, of which waited for: 7 -> 7; matrix products, arithmetic and copies ran while one was open for 5% -> 3% of each run, Pallas kernels for 0% -> 0%
where the time goes in v1:
time: 675 us; the launch traced here: 674 us
  waiting for transfers between devices  333 us (49%)
  blocking collectives  257 us (38%)
  other arithmetic  24.2 us (4%)
  matrix products  23.4 us (3%)
  local copies, waits for them, and re-layouts  21.1 us (3%)
  between operations  14.2 us (2%)
    all_gather x2, waiting for transfers between devices, on_device(): stream = stream + 0.5 * jnp.sum(lax.all_gather(partial_out, 'fs'), axis=0)  184 us
    all_gather x4, waiting for transfers between devices, on_device(): lax.all_gather(as_sent(shaped), 'tp', axis=1, tiled=True)  100 us
    all_to_all x1, blocking collectives, on_device(): lax.all_to_all(spread[2], 'fs', split_axis=1, concat_axis=0, tiled=True)  61.6 us
    all_to_all x1, blocking collectives, on_device(): lax.all_to_all(spread[3], 'fs', split_axis=1, concat_axis=0, tiled=True)  58 us
    all_gather x1, waiting for transfers between devices, on_device(): lax.all_gather(downs[1], 'tp', axis=1, tiled=True)  31.7 us
    all_to_all x1, blocking collectives, on_device(): lax.all_to_all(spread[0], 'fs', split_axis=1, concat_axis=0, tiled=True)  30.3 us
    all_to_all x1, blocking collectives, on_device(): lax.all_to_all(spread[1], 'fs', split_axis=1, concat_axis=0, tiled=True)  28.6 us
    all_to_all x1, blocking collectives, on_device(): lax.all_to_all(folded[1], 'tp', split_axis=0, concat_axis=1, tiled=True)  26.5 us
  transfers between devices with their start and end apart: 8, of which 7 were waited for; matrix products, arithmetic and copies ran while one was open for 3% of the time, Pallas kernels for 0%

profile of v1, /device:TPU:0, one launch (start us, length us, event | category | flops | bytes accessed | tf_op | source)
XLA Modules:
  0.0 673.9 jit_solution(2388162379954160333)
XLA Ops:
  7.2 2.5 multiply_convert_fusion.4
  9.7 18.5 %all_to_all.116 = bf16[4,128,1024]{2,1,0:T(8,128)(2,1)S(1)} all-to-all(bf16[4,128,1024]{2,1,0:T(8,128)(2,1)S(1)} %bitcast.46), channel_id=1, replica_groups=mesh['grp'=2,'fs'=4,'tp'=4] {'tp'}, dimensions={0} | all-to-all | bytes 2097152 | tf_op jit(solution)/shard_map/all_to_all | solution.py:48
  28.2 30.3 %all_to_all.117 = bf16[128,4,1024]{2,0,1:T(8,128)(2,1)} all-to-all(bf16[128,4,1024]{2,0,1:T(8,128)(2,1)S(1)} %bitcast.40), channel_id=1, replica_groups=mesh['grp'=2,'fs'=4,'tp'=4] {'fs'}, dimensions={1} | all-to-all | bytes 2097152 | tf_op jit(solution)/shard_map/all_to_all | solution.py:54
  59.7 26.5 %all_to_all.118 = bf16[4,128,1024]{2,1,0:T(8,128)(2,1)S(1)} all-to-all(bf16[4,128,1024]{2,1,0:T(8,128)(2,1)S(1)} %bitcast.44), channel_id=1, replica_groups=mesh['grp'=2,'fs'=4,'tp'=4] {'tp'}, dimensions={0} | all-to-all | bytes 2097152 | tf_op jit(solution)/shard_map/all_to_all | solution.py:49
  86.2 28.6 %all_to_all.119 = bf16[128,4,1024]{2,0,1:T(8,128)(2,1)} all-to-all(bf16[128,4,1024]{2,0,1:T(8,128)(2,1)S(1)} %bitcast.41), channel_id=1, replica_groups=mesh['grp'=2,'fs'=4,'tp'=4] {'fs'}, dimensions={1} | all-to-all | bytes 2097152 | tf_op jit(solution)/shard_map/all_to_all | solution.py:55
  115.2 3.5 fusion.10
  118.7 16.8 %all-gather.15.cloned.1.call-done = bf16[1024,2048]{1,0:T(8,128)(2,1)} async-done(((bf16[1024,512]{1,0:T(8,128)(2,1)}), bf16[1024,2048]{1,0:T(8,128)(2,1)}) %all-gather.15.cloned.1.call-update) | async-done | bytes 4194320 | tf_op jit(solution)/shard_map/all_gather | solution.py:70
  135.5 36.1 %all-gather.13.cloned.1.call-done = bf16[4,512,1024]{2,1,0:T(8,128)(2,1)} async-done(((bf16[4,128,1024]{2,1,0:T(8,128)(2,1)}), bf16[4,512,1024]{2,1,0:T(8,128)(2,1)}) %all-gather.13.cloned.1.call-update) | async-done | bytes 4194320 | tf_op jit(solution)/shard_map/all_gather | solution.py:65
  171.5 7.4 %fusion.5 = f32[256,2048]{1,0:T(8,128)} fusion(bf16[1024,2048]{1,0:T(8,128)(2,1)} %all-gather.15.cloned.1.call-done, bf16[2048,1024]{1,0:T(8,128)(2,1)} %bitcast.30, f32[256,1024]{1,0:T(8,128)S(1)} %fusion.10, bf16[256,2048]{1,0:T(8,128)(2,1)S(1)} %copy-done, f32[256]{0:T(256)S(1)} %add_rsqrt_fusion.1), kind=kOutput, calls=%fused_computation.17 | convolution fusion | flops 2150629376 | bytes 12583936 | tf_op jit(solution)/shard_map/dot_general | solution.py:78
  179.6 2.5 multiply_convert_fusion.1
  182.1 16.9 %all_to_all.120 = bf16[4,128,1024]{2,1,0:T(8,128)(2,1)S(1)} all-to-all(bf16[4,128,1024]{2,1,0:T(8,128)(2,1)S(1)} %bitcast.47), channel_id=1, replica_groups=mesh['grp'=2,'fs'=4,'tp'=4] {'tp'}, dimensions={0} | all-to-all | bytes 2097152 | tf_op jit(solution)/shard_map/all_to_all | solution.py:50
  199.0 61.6 %all_to_all.121 = bf16[128,4,1024]{2,0,1:T(8,128)(2,1)} all-to-all(bf16[128,4,1024]{2,0,1:T(8,128)(2,1)S(1)} %bitcast.42), channel_id=1, replica_groups=mesh['grp'=2,'fs'=4,'tp'=4] {'fs'}, dimensions={1} | all-to-all | bytes 2097152 | tf_op jit(solution)/shard_map/all_to_all | solution.py:56
  260.7 2.7 convert_element_type.46
  263.4 17.0 %all_to_all.122 = bf16[4,128,1024]{2,1,0:T(8,128)(2,1)S(1)} all-to-all(bf16[4,128,1024]{2,1,0:T(8,128)(2,1)S(1)} %bitcast.45), channel_id=1, replica_groups=mesh['grp'=2,'fs'=4,'tp'=4] {'tp'}, dimensions={0} | all-to-all | bytes 2097152 | tf_op jit(solution)/shard_map/all_to_all | solution.py:51
  280.4 58.0 %all_to_all.123 = bf16[128,4,1024]{2,0,1:T(8,128)(2,1)} all-to-all(bf16[128,4,1024]{2,0,1:T(8,128)(2,1)S(1)} %bitcast.43), channel_id=1, replica_groups=mesh['grp'=2,'fs'=4,'tp'=4] {'fs'}, dimensions={1} | all-to-all | bytes 2097152 | tf_op jit(solution)/shard_map/all_to_all | solution.py:57
  338.7 34.7 %all-gather.23.cloned.1.call-done = f32[1024,2048]{1,0:T(8,128)} async-done(((f32[256,2048]{1,0:T(8,128)}), f32[1024,2048]{1,0:T(8,128)}) %all-gather.23.cloned.1.call-update) | async-done | bytes 8388624 | tf_op jit(solution)/shard_map/all_gather | solution.py:79
  373.3 4.4 reduce_sum.37
  379.5 27.9 %all-gather.17.cloned.1.call-done = bf16[4,512,1024]{2,1,0:T(8,128)(2,1)} async-done(((bf16[4,128,1024]{2,1,0:T(8,128)(2,1)}), bf16[4,512,1024]{2,1,0:T(8,128)(2,1)}) %all-gather.17.cloned.1.call-update) | async-done | bytes 4194320 | tf_op jit(solution)/shard_map/all_gather | solution.py:65
  407.4 4.7 fusion.14
  412.1 31.7 %all-gather.21.cloned.1.call-done = bf16[1024,2048]{1,0:T(8,128)(2,1)} async-done(((bf16[1024,512]{1,0:T(8,128)(2,1)}), bf16[1024,2048]{1,0:T(8,128)(2,1)}) %all-gather.21.cloned.1.call-update) | async-done | bytes 4194320 | tf_op jit(solution)/shard_map/all_gather | solution.py:71
  443.9 36.0 %all-gather.19.cloned.1.call-done = bf16[4,512,1024]{2,1,0:T(8,128)(2,1)} async-done(((bf16[4,128,1024]{2,1,0:T(8,128)(2,1)}), bf16[4,512,1024]{2,1,0:T(8,128)(2,1)}) %all-gather.19.cloned.1.call-update) | async-done | bytes 4194320 | tf_op jit(solution)/shard_map/all_gather | solution.py:65
  479.9 7.9 %fusion.4 = f32[256,2048]{1,0:T(8,128)} fusion(bf16[1024,2048]{1,0:T(8,128)(2,1)} %all-gather.21.cloned.1.call-done, bf16[256,2048]{1,0:T(8,128)(2,1)} %multiply_convert_fusion.2, bf16[2048,1024]{1,0:T(8,128)(2,1)} %bitcast.34, f32[256,1024]{1,0:T(8,128)} %fusion.14), kind=kOutput, calls=%fused_computation.16 | convolution fusion | flops 2149056512 | bytes 12582912 | tf_op jit(solution)/shard_map/dot_general | solution.py:78
  487.8 149.8 %all-gather.25.cloned.1.call-done = f32[1024,2048]{1,0:T(8,128)} async-done(((f32[256,2048]{1,0:T(8,128)}), f32[1024,2048]{1,0:T(8,128)}) %all-gather.25.cloned.1.call-update) | async-done | bytes 8388624 | tf_op jit(solution)/shard_map/all_gather | solution.py:79
  637.6 5.7 reduce_sum.39
  643.3 3.2 add_convert_fusion
  646.5 2.1 copy.22
  650.2 2.1 copy.23
  653.9 2.1 copy.24
  656.1 1.6 copy-done.4
  657.6 2.1 copy.25
  661.3 2.1 copy.26
  665.0 2.0 copy.27
  (40 shorter events, 10.7 us)
Async XLA Ops:
  7.2 108.0 %all-gather.11.cloned.1.call-start = ((), (), s32[]{:S(2)}) async-start(), calls=%async_computation.8 | async-start | bytes 5242880 | tf_op jit(solution)/shard_map/all_gather | solution.py:65
  28.2 30.3 %copy-start.7 = (f32[1024,512]{1,0:T(8,128)S(1)}, f32[1024,512]{1,0:T(8,128)}, u32[]{:S(2)}) copy-start(f32[1024,512]{1,0:T(8,128)} %param.13) | copy-start | bytes 6291460
  58.5 77.0 %all-gather.15.cloned.1.call-start = ((), (), s32[]{:S(2)}) async-start(), calls=%async_computation.10 | async-start | bytes 5242880 | tf_op jit(solution)/shard_map/all_gather | solution.py:70
  59.7 111.8 %all-gather.13.cloned.1.call-start = ((), (), s32[]{:S(2)}) async-start(), calls=%async_computation.9 | async-start | bytes 5242880 | tf_op jit(solution)/shard_map/all_gather | solution.py:65
  86.2 28.7 %copy-start = (bf16[256,2048]{1,0:T(8,128)(2,1)S(1)}, bf16[256,2048]{1,0:T(8,128)(2,1)}, u32[]{:S(2)}) copy-start(bf16[256,2048]{1,0:T(8,128)(2,1)} %param.9) | copy-start | bytes 3145732
  114.8 258.5 %all-gather.23.cloned.1.call-start = ((), (), s32[]{:S(2)}) async-start(), calls=%async_computation.14 | async-start | bytes 10485760 | tf_op jit(solution)/shard_map/all_gather | solution.py:79
  178.9 0.7 copy-start.8
  178.9 228.4 %all-gather.17.cloned.1.call-start = ((), (), s32[]{:S(2)}) async-start(), calls=%async_computation.11 | async-start | bytes 5242880 | tf_op jit(solution)/shard_map/all_gather | solution.py:65
  260.6 183.3 %all-gather.21.cloned.1.call-start = ((), (), s32[]{:S(2)}) async-start(), calls=%async_computation.13 | async-start | bytes 5242880 | tf_op jit(solution)/shard_map/all_gather | solution.py:71
  263.4 216.5 %all-gather.19.cloned.1.call-start = ((), (), s32[]{:S(2)}) async-start(), calls=%async_computation.12 | async-start | bytes 5242880 | tf_op jit(solution)/shard_map/all_gather | solution.py:65
  338.4 299.1 %all-gather.25.cloned.1.call-start = ((), (), s32[]{:S(2)}) async-start(), calls=%async_computation.15 | async-start | bytes 10485760 | tf_op jit(solution)/shard_map/all_gather | solution.py:79
  643.3 3.2 copy-start.1
  646.5 3.7 copy-start.3
  650.2 3.7 copy-start.2
  653.9 3.7 copy-start.4
  657.6 3.7 copy-start.6
  661.3 3.7 copy-start.5
Sparse Core Ops, SparseCore 0:
  58.6 42.0 all-gather.10
  102.8 32.6 all-gather.14
  137.0 34.4 all-gather.12
  179.1 194.2 all-gather.22
  374.8 32.5 all-gather.16
  409.4 34.4 all-gather.20
  445.4 34.4 all-gather.18
  487.9 149.6 all-gather.24
